TPU v7x, 32 devices: a whole 2x2x4 slice. The times are simulated.
32 devices in a mesh: ep: 8 (over z, x), tp: 4 (over y, core).
Axes of the slice: x: 2, y: 2, z: 4, core: 2. Of those that a mesh axis runs over, the one named last changes fastest.
Arguments:
- tokens: bfloat16 [192, 2048], P('ep'), may hold values from -12 to 12
- state: float32 [192, 16, 128, 256], P('ep', 'tp'), may hold values from -6 to 6
- w_query: bfloat16 [2048, 2048], P(None, 'tp'), may hold values from -0.125 to 0.125
- w_key: bfloat16 [2048, 2048], P(None, 'tp'), may hold values from -0.125 to 0.125
- w_value: bfloat16 [2048, 4096], P(None, 'tp'), may hold values from -0.125 to 0.125
- w_outgate: bfloat16 [2048, 4096], P(None, 'tp'), may hold values from -0.125 to 0.125
- decay_down: bfloat16 [2048, 16], replicated, may hold values from -0.125 to 0.125
- decay_up: bfloat16 [16, 2048], P(None, 'tp'), may hold values from -9 to 9
- decay_bias: float32 [2048], P('tp'), may hold values from -6 to 4
- head_gain: float32 [256], replicated, may hold values from 0.1 to 1.9
- w_output: bfloat16 [4096, 2048], P('tp'), may hold values from -0.09375 to 0.09375
- norm1_gain: float32 [2048], P('tp'), may hold values from 0.1 to 1.9
- route_ids: int32 [192, 6], P('ep'), may hold values from 0 to 31, all different within a row; in each aligned block of 24 rows (0 to 23, 24 to 47, ...) at most 5 rows name the same one
- route_weight: float32 [192, 6], P('ep'), may hold values from 0.1 to 1
- exp_gate: bfloat16 [32, 2048, 512], P('ep', 'tp'), may hold values from -0.125 to 0.125
- exp_up: bfloat16 [32, 2048, 512], P('ep', 'tp'), may hold values from -0.125 to 0.125
- exp_down: bfloat16 [32, 512, 2048], P('ep', None, 'tp'), may hold values from -0.25 to 0.25
- sh_gate: bfloat16 [2048, 512], P('tp'), may hold values from -0.125 to 0.125
- sh_up: bfloat16 [2048, 512], P('tp'), may hold values from -0.125 to 0.125
- sh_down: bfloat16 [512, 2048], P(None, 'tp'), may hold values from -0.25 to 0.25
- norm2_gain: float32 [2048], P('tp'), may hold values from 0.1 to 1.9
Outputs:
- layer_out: bfloat16 [192, 2048], P('ep', 'tp')
Inputs may be any that keep to these rules, and one draw needn't show every extreme that they name: `route_ids`: each row names 6 different experts. Among the rows of one index of ep (aligned blocks of 24 rows) no expert is named by more than 5 rows, and in some blocks one expert is named by exactly 5.
All inputs are finite; a program needn't handle non-finite values.
Results may differ from a plain program's by a relative error of at most 0.02.
Values may be sent and summed in bfloat16 or wider, within the bound.
A program may use at most 64 MiB of HBM per device.

v0:
```python
import jax
import jax.numpy as jnp
from jax import lax
from jax.sharding import PartitionSpec as P

res_scale = 2.0**0.5
decay_tau = 16.0
norm_eps = 1e-05


def settle(values):
    return lax.optimization_barrier(values.astype(jnp.bfloat16)).astype(jnp.float32)


def project(left, right):
    return jnp.dot(left, right, preferred_element_type=jnp.float32)


def apply_norm(values, sums, squares, width, gain):
    mean_val = sums[:, None] / width
    spread = squares[:, None] / width - mean_val * mean_val
    return (values - mean_val) * lax.rsqrt(spread + norm_eps) * gain


def per_device(
    tokens,
    state,
    w_query,
    w_key,
    w_value,
    w_outgate,
    decay_down,
    decay_up,
    decay_bias,
    head_gain,
    w_output,
    norm1_gain,
    route_ids,
    route_weight,
    exp_gate,
    exp_up,
    exp_down,
    sh_gate,
    sh_up,
    sh_down,
    norm2_gain,
):
    row_count, width = tokens.shape
    head_count, key_dim, val_dim = (state.shape[1], state.shape[2], state.shape[3])
    tp_count = lax.axis_size("tp")
    ep_count = lax.axis_size("ep")
    col_count = width // tp_count
    col_start = lax.axis_index("tp") * col_count
    queries = settle(project(tokens, w_query)).reshape(
        row_count, head_count, key_dim
    ) * key_dim ** (-0.5)
    key_rows = settle(project(tokens, w_key)).reshape(row_count, head_count, key_dim)
    values = settle(project(tokens, w_value)).reshape(row_count, head_count, val_dim)
    gate_pre = settle(project(tokens, w_outgate)).reshape(row_count, head_count, val_dim)
    decay_low = lax.optimization_barrier(project(tokens, decay_down).astype(jnp.bfloat16))
    log_decay = (jax.nn.log_sigmoid(project(decay_low, decay_up) + decay_bias) / decay_tau).reshape(
        row_count, head_count, key_dim
    )
    carried = jnp.einsum(
        "bhk,bhkv->bhv", queries * jnp.exp(log_decay), state, precision=lax.Precision.HIGHEST
    )
    attended = carried + jnp.sum(queries * key_rows, -1, keepdims=True) * values
    inv_norm = lax.rsqrt(jnp.mean(attended * attended, -1, keepdims=True) + norm_eps)
    head_out = (
        (attended * inv_norm * head_gain * jax.nn.silu(gate_pre))
        .astype(jnp.bfloat16)
        .reshape(row_count, head_count * val_dim)
    )
    partial_out = project(head_out, w_output)
    mixed = settle(
        lax.psum_scatter(
            partial_out.astype(jnp.bfloat16), "tp", scatter_dimension=1, tiled=True
        ).astype(jnp.float32)
    )
    own_tokens = lax.dynamic_slice_in_dim(tokens, col_start, col_count, 1).astype(jnp.float32)
    own_resid = res_scale * own_tokens + mixed
    first_sums, first_squares = lax.psum(
        (jnp.sum(own_resid, -1), jnp.sum(own_resid * own_resid, -1)), "tp"
    )
    normed_mid = apply_norm(own_resid, first_sums, first_squares, width, norm1_gain)
    normed_mid = lax.optimization_barrier(normed_mid.astype(jnp.bfloat16))
    top_count = route_ids.shape[1]
    local_count = exp_gate.shape[0]
    expert_count = local_count * ep_count
    capacity = max(2, row_count * top_count // expert_count + 1)
    flat_ids = route_ids.reshape(row_count * top_count)
    onehot = (flat_ids[:, None] == jnp.arange(expert_count, dtype=jnp.int32)[None, :]).astype(
        jnp.int32
    )
    ranks = jnp.sum((jnp.cumsum(onehot, 0) - 1) * onehot, 1)
    slots = flat_ids * capacity + ranks
    placement = (
        slots[:, None] == jnp.arange(expert_count * capacity, dtype=jnp.int32)[None, :]
    ).astype(jnp.bfloat16)
    pair_rows = jnp.repeat(normed_mid, top_count, axis=0)
    outgoing = jnp.einsum(
        "ps,pc->sc", placement, pair_rows, preferred_element_type=jnp.float32
    ).astype(jnp.bfloat16)
    outgoing = outgoing.reshape(ep_count, local_count, capacity, col_count)
    incoming = lax.all_to_all(outgoing, "ep", split_axis=0, concat_axis=0, tiled=True)
    gate_part = jnp.einsum("secd,edf->secf", incoming, exp_gate, preferred_element_type=jnp.float32)
    up_part = jnp.einsum("secd,edf->secf", incoming, exp_up, preferred_element_type=jnp.float32)
    shared_gate_part = project(normed_mid, sh_gate)
    shared_up_part = project(normed_mid, sh_up)
    gate_sum, up_sum, shared_gate_sum, shared_up_sum = (
        lax.psum(gate_part.astype(jnp.bfloat16), "tp").astype(jnp.float32),
        lax.psum(up_part.astype(jnp.bfloat16), "tp").astype(jnp.float32),
        lax.psum(shared_gate_part.astype(jnp.bfloat16), "tp").astype(jnp.float32),
        lax.psum(shared_up_part.astype(jnp.bfloat16), "tp").astype(jnp.float32),
    )
    inner = (jax.nn.silu(settle(gate_sum)) * settle(up_sum)).astype(jnp.bfloat16)
    shared_inner = (jax.nn.silu(settle(shared_gate_sum)) * settle(shared_up_sum)).astype(
        jnp.bfloat16
    )
    expert_out = jnp.einsum(
        "secf,efd->secd", inner, exp_down, preferred_element_type=jnp.float32
    ).astype(jnp.bfloat16)
    returned = lax.all_to_all(expert_out, "ep", split_axis=0, concat_axis=0, tiled=True)
    picked = jnp.einsum(
        "ps,sc->pc",
        placement,
        returned.reshape(expert_count * capacity, col_count),
        preferred_element_type=jnp.float32,
    )
    routed = jnp.sum(picked.reshape(row_count, top_count, col_count) * route_weight[:, :, None], 1)
    mixture = routed + project(shared_inner, sh_down)
    out_resid = res_scale * normed_mid.astype(jnp.float32) + mixture
    last_sums, last_squares = lax.psum(
        (jnp.sum(out_resid, -1), jnp.sum(out_resid * out_resid, -1)), "tp"
    )
    return apply_norm(out_resid, last_sums, last_squares, width, norm2_gain).astype(jnp.bfloat16)


def solution(mesh):
    in_specs = (
        P("ep", None),
        P("ep", "tp", None, None),
        P(None, "tp"),
        P(None, "tp"),
        P(None, "tp"),
        P(None, "tp"),
        P(),
        P(None, "tp"),
        P("tp"),
        P(),
        P("tp", None),
        P("tp"),
        P("ep", None),
        P("ep", None),
        P("ep", "tp", None),
        P("ep", "tp", None),
        P("ep", None, "tp"),
        P("tp", None),
        P("tp", None),
        P(None, "tp"),
        P("tp"),
    )
    out_specs = P("ep", "tp")
    return jax.shard_map(
        per_device, mesh=mesh, in_specs=in_specs, out_specs=out_specs, check_vma=False
    )
```

profile of v0, /device:TPU:0, one launch (start us, length us, event | category | flops | bytes accessed | tf_op | source)
XLA Modules:
  0.0 142.7 jit_solution(752916315707150363)
XLA Ops:
  6.6 2.2 %convolution_convert_fusion.5 = bf16[24,512]{1,0:T(8,128)(2,1)S(1)} fusion(bf16[24,2048]{1,0:T(8,128)(2,1)} %param.21, bf16[2048,512]{1,0:T(8,128)(2,1)} %param.23), kind=kOutput, calls=%fused_computation.23 | convolution fusion | flops 50343936 | bytes 2220032 | tf_op jit(solution)/shard_map/dot_general | solution.py:16
  8.9 0.2 fusion.49
  9.2 2.0 %convolution_convert_fusion.4 = bf16[24,512]{1,0:T(8,128)(2,1)S(1)} fusion(bf16[24,2048]{1,0:T(8,128)(2,1)S(1)} %copy-done.1, bf16[2048,512]{1,0:T(8,128)(2,1)} %param.24), kind=kOutput, calls=%fused_computation.22 | convolution fusion | flops 50343936 | bytes 2220032 | tf_op jit(solution)/shard_map/dot_general | solution.py:16
  11.2 2.8 %convolution_convert_fusion.3 = bf16[24,1024]{1,0:T(8,128)(2,1)S(1)} fusion(bf16[24,2048]{1,0:T(8,128)(2,1)S(1)} %copy-done.1, bf16[2048,1024]{1,0:T(8,128)(2,1)} %param.25), kind=kOutput, calls=%fused_computation.17 | convolution fusion | flops 100687872 | bytes 4341760 | tf_op jit(solution)/shard_map/dot_general | solution.py:16
  14.1 8.6 %fusion.59 = f32[24,4,1,256]{3,2,1,0:T(1,128)S(1)} fusion(f32[24,4,128,1]{2,3,1,0:T(1,128)S(1)} %bitcast.80, f32[24,4,128,256]{3,2,1,0:T(8,128)} %param.22), kind=kOutput, calls=%fused_computation.88 | convolution fusion | flops 37748736 | bytes 12730368 | tf_op jit(solution)/shard_map/bhk,bhkv->bhv/dot_general | solution.py:64
  22.8 0.2 multiply_reduce_fusion
  23.0 2.8 %convolution_convert_fusion.2 = bf16[24,1024]{1,0:T(8,128)(2,1)S(1)} fusion(bf16[24,2048]{1,0:T(8,128)(2,1)S(1)} %copy-done.1, bf16[2048,1024]{1,0:T(8,128)(2,1)} %param.26), kind=kOutput, calls=%fused_computation.16 | convolution fusion | flops 100687872 | bytes 4341760 | tf_op jit(solution)/shard_map/dot_general | solution.py:16
  26.1 3.5 %convolution_convert_fusion = bf16[24,2048]{1,0:T(8,128)(2,1)} fusion(bf16[24,1024]{1,0:T(8,128)(2,1)S(1)} %bitcast.81, bf16[1024,2048]{1,0:T(8,128)(2,1)} %param.31), kind=kOutput, calls=%fused_computation | convolution fusion | flops 100712448 | bytes 4341760 | tf_op jit(solution)/shard_map/dot_general | solution.py:16
  29.9 0.6 reduce-window.6
  30.4 0.2 slice_reduce_fusion
  30.8 21.4 %reduce-scatter.2.cloned.1.call-done = bf16[24,512]{1,0:T(8,128)(2,1)} async-done(((bf16[24,2048]{1,0:T(8,128)(2,1)}), bf16[24,512]{1,0:T(8,128)(2,1)}) %reduce-scatter.2.cloned.1.call-update) | async-done | bytes 24592 | tf_op jit(solution)/shard_map/reduce_scatter | solution.py:76
  52.2 0.9 fusion.51
  53.0 5.8 %all-reduce.2 = (f32[24]{0:T(128)S(1)}, f32[24]{0:T(128)S(1)}) all-reduce(f32[24]{0:T(128)S(1)} %get-tuple-element.6, f32[24]{0:T(128)S(1)} %get-tuple-element.5), channel_id=1, replica_groups=mesh['ep'=8,'tp'=4] {'tp'}, use_global_device_ids=true, to_apply=%region_6.7 | all-reduce | flops 48 | bytes 384 | tf_op jit(solution)/shard_map/psum | solution.py:82
  58.8 0.8 multiply_convert_fusion.1
  59.7 0.3 convolution_convert_fusion.1
  60.1 0.7 copy.52
  60.9 5.7 %all-to-all-start = ((bf16[8,4,5,512]{3,1,2,0:T(4,128)(2,1)}), bf16[8,4,5,512]{3,1,2,0:T(4,128)(2,1)S(1)}, u32[]{:S(2)}, u32[]{:S(2)}) async-start(bf16[8,4,5,512]{3,1,2,0:T(4,128)(2,1)} %copy.52), calls=%async_computation.1 | async-start | bytes 327680 | tf_op jit(solution)/shard_map/all_to_all | solution.py:105
  66.7 7.3 %all-to-all-done = bf16[8,4,5,512]{3,1,2,0:T(4,128)(2,1)S(1)} async-done(((bf16[8,4,5,512]{3,1,2,0:T(4,128)(2,1)}), bf16[8,4,5,512]{3,1,2,0:T(4,128)(2,1)S(1)}, u32[]{:S(2)}, u32[]{:S(2)}) %all-to-all-start) | async-done | bytes 163872 | tf_op jit(solution)/shard_map/all_to_all | solution.py:105
  74.1 1.1 fusion.19
  75.2 0.6 copy-done.2
  75.8 1.1 fusion.22
  76.9 29.9 %all-reduce.7.cloned.1.call-done = (bf16[8,4,5,512]{3,0,2,1:T(8,128)(2,1)}, bf16[8,4,5,512]{3,0,2,1:T(8,128)(2,1)}) async-done(((bf16[8,4,5,512]{3,0,2,1:T(8,128)(2,1)}, bf16[8,4,5,512]{3,0,2,1:T(8,128)(2,1)}), (bf16[8,4,5,512]{3,0,2,1:T(8,128)(2,1)}, bf16[8,4,5,512]{3,0,2,1:T(8,128)(2,1)})) %all-reduce.7.cloned.1.call-update) | async-done | bytes 327696 | tf_op jit(solution)/shard_map/psum | solution.py:112
  106.8 2.2 %fusion.16 = bf16[8,4,5,512]{3,0,2,1:T(8,128)(2,1)S(1)} fusion(bf16[4,512,512]{2,1,0:T(8,128)(2,1)} %param.37, bf16[8,4,5,512]{3,0,2,1:T(8,128)(2,1)} %get-tuple-element.15, bf16[8,4,5,512]{3,0,2,1:T(8,128)(2,1)} %get-tuple-element.16), kind=kOutput, calls=%fused_computation.13 | convolution fusion | flops 84623360 | bytes 2588672 | tf_op jit(solution)/shard_map/secf,efd->secd/dot_general | solution.py:120
  109.0 0.7 copy.55
  109.7 5.5 %all-to-all-start.1 = ((bf16[8,4,5,512]{3,1,2,0:T(4,128)(2,1)}), bf16[8,4,5,512]{3,1,2,0:T(4,128)(2,1)S(1)}, u32[]{:S(2)}, u32[]{:S(2)}) async-start(bf16[8,4,5,512]{3,1,2,0:T(4,128)(2,1)} %copy.55), calls=%async_computation.2 | async-start | bytes 327680 | tf_op jit(solution)/shard_map/all_to_all | solution.py:123
  115.2 0.2 convolution_convert_fusion.6
  115.4 1.2 convolution_convert_fusion.7
  116.7 10.9 %all-reduce.3 = (bf16[24,512]{1,0:T(8,128)(2,1)S(1)}, bf16[24,512]{1,0:T(8,128)(2,1)S(1)}) all-reduce(bf16[24,512]{1,0:T(8,128)(2,1)S(1)} %convolution_convert_fusion.6, bf16[24,512]{1,0:T(8,128)(2,1)S(1)} %convolution_convert_fusion.7), channel_id=1, replica_groups=mesh['ep'=8,'tp'=4] {'tp'}, use_global_device_ids=true, to_apply=%region_14.15 | all-reduce | flops 24576 | bytes 98304 | tf_op jit(solution)/shard_map/psum | solution.py:114
  127.7 0.2 fusion.15
  127.9 1.3 fusion.58
  129.3 5.9 %all-reduce.1 = (f32[24]{0:T(128)S(1)}, f32[24]{0:T(128)S(1)}) all-reduce(f32[24]{0:T(128)S(1)} %get-tuple-element.8, f32[24]{0:T(128)S(1)} %get-tuple-element.7), channel_id=1, replica_groups=mesh['ep'=8,'tp'=4] {'tp'}, use_global_device_ids=true, to_apply=%region_18.19 | all-reduce | flops 48 | bytes 384 | tf_op jit(solution)/shard_map/psum | solution.py:133
  135.2 0.7 multiply_convert_fusion
  (57 shorter events, 1.6 us)
Async XLA Ops:
  6.5 67.6 %copy-start = (bf16[4,512,512]{2,1,0:T(8,128)(2,1)S(1)}, bf16[4,512,512]{2,1,0:T(8,128)(2,1)}, u32[]{:S(2)}) copy-start(bf16[4,512,512]{2,1,0:T(8,128)(2,1)} %param.36) | copy-start | bytes 6291460
  6.5 2.2 %copy-start.1 = (bf16[24,2048]{1,0:T(8,128)(2,1)S(1)}, bf16[24,2048]{1,0:T(8,128)(2,1)}, u32[]{:S(2)}) copy-start(bf16[24,2048]{1,0:T(8,128)(2,1)} %param.21) | copy-start | bytes 294916
  6.5 2.2 %copy-start.4 = (bf16[2048,16]{0,1:T(8,128)(2,1)S(1)}, bf16[2048,16]{0,1:T(8,128)(2,1)}, u32[]{:S(2)}) copy-start(bf16[2048,16]{0,1:T(8,128)(2,1)} %param.27) | copy-start | bytes 196612
  6.5 2.4 %copy-start.9 = (bf16[16,512]{1,0:T(8,128)(2,1)S(1)}, bf16[16,512]{1,0:T(8,128)(2,1)}, u32[]{:S(2)}) copy-start(bf16[16,512]{1,0:T(8,128)(2,1)} %param.28) | copy-start | bytes 49156
  6.5 2.4 %copy-start.11 = (f32[512]{0:T(512)S(1)}, f32[512]{0:T(512)}, u32[]{:S(2)}) copy-start(f32[512]{0:T(512)} %param.29) | copy-start | bytes 6148
  6.5 45.6 %reduce-scatter.2.cloned.1.call-start = ((), (), s32[]{:S(2)}) async-start(), calls=%async_computation.3 | async-start | bytes 122880 | tf_op jit(solution)/shard_map/reduce_scatter | solution.py:76
  23.0 2.9 %copy-start.8 = (f32[256]{0:T(256)S(1)}, f32[256]{0:T(256)}, u32[]{:S(2)}) copy-start(f32[256]{0:T(256)} %param.30) | copy-start | bytes 3076
  26.1 3.5 %copy-start.5 = (s32[24,6]{0,1:T(8,128)S(1)}, s32[24,6]{0,1:T(8,128)}, u32[]{:S(2)}) copy-start(s32[24,6]{0,1:T(8,128)} %param.33) | copy-start | bytes 1732
  26.1 32.7 %copy-start.6 = (f32[512]{0:T(512)S(1)}, f32[512]{0:T(512)}, u32[]{:S(2)}) copy-start(f32[512]{0:T(512)} %param.32) | copy-start | bytes 6148
  60.9 13.2 %all-to-all-start = ((bf16[8,4,5,512]{3,1,2,0:T(4,128)(2,1)}), bf16[8,4,5,512]{3,1,2,0:T(4,128)(2,1)S(1)}, u32[]{:S(2)}, u32[]{:S(2)}) async-start(bf16[8,4,5,512]{3,1,2,0:T(4,128)(2,1)} %copy.52), calls=%async_computation.1 | async-start | bytes 327680 | tf_op jit(solution)/shard_map/all_to_all | solution.py:105
  66.5 40.2 %all-reduce.7.cloned.1.call-start = ((), (), s32[]{:S(2)}) async-start(), calls=%async_computation.4 | async-start | bytes 655360 | tf_op jit(solution)/shard_map/psum | solution.py:112
  74.1 1.7 %copy-start.2 = (bf16[4,512,512]{2,1,0:T(8,128)(2,1)S(1)}, bf16[4,512,512]{2,1,0:T(8,128)(2,1)}, u32[]{:S(2)}) copy-start(bf16[4,512,512]{2,1,0:T(8,128)(2,1)} %param.35) | copy-start | bytes 6291460
  76.8 38.4 %copy-start.3 = (bf16[512,512]{1,0:T(8,128)(2,1)S(1)}, bf16[512,512]{1,0:T(8,128)(2,1)}, u32[]{:S(2)}) copy-start(bf16[512,512]{1,0:T(8,128)(2,1)} %param.39) | copy-start | bytes 1572868
  106.8 20.9 %copy-start.10 = (f32[24,6]{0,1:T(8,128)S(1)}, f32[24,6]{0,1:T(8,128)}, u32[]{:S(2)}) copy-start(f32[24,6]{0,1:T(8,128)} %param.34) | copy-start | bytes 1732
  109.0 26.2 %copy-start.7 = (f32[512]{0:T(512)S(1)}, f32[512]{0:T(512)}, u32[]{:S(2)}) copy-start(f32[512]{0:T(512)} %param.41) | copy-start | bytes 6148
  109.7 17.8 %all-to-all-start.1 = ((bf16[8,4,5,512]{3,1,2,0:T(4,128)(2,1)}), bf16[8,4,5,512]{3,1,2,0:T(4,128)(2,1)S(1)}, u32[]{:S(2)}, u32[]{:S(2)}) async-start(bf16[8,4,5,512]{3,1,2,0:T(4,128)(2,1)} %copy.55), calls=%async_computation.2 | async-start | bytes 327680 | tf_op jit(solution)/shard_map/all_to_all | solution.py:123
Sparse Core Ops, SparseCore 0:
  29.7 22.3 reduce-scatter.1
  77.0 29.7 all-reduce.6
where the time goes:
time: 143 us
  waiting for transfers between devices  58.6 us (41%)
  matrix products  29.9 us (21%)
  blocking collectives  22.5 us (16%)
  between operations  13.7 us (10%)
  starting transfers between devices  11.3 us (8%)
  other arithmetic  3.59 us (3%)
  local copies, waits for them, and re-layouts  3.1 us (2%)
    psum x1, waiting for transfers between devices, per_device(): lax.psum(up_part.astype(jnp.bfloat16), 'tp').astype(jnp.float32)  29.9 us
    reduce_scatter x1, waiting for transfers between devices, per_device(): lax.psum_scatter(partial_out.astype(jnp.bfloat16), 'tp', scatter_dimensio...  21.4 us
    dot_general x10, matrix products, project(): return jnp.dot(left, right, preferred_element_type=jnp.float32)  16.4 us
    psum x1, blocking collectives, per_device(): lax.psum(shared_up_part.astype(jnp.bfloat16), 'tp').astype(jnp.float32)  10.9 us
    dot_general x1, matrix products, per_device(): jnp.einsum('bhk,bhkv->bhv', queries * jnp.exp(log_decay), state, precisio...  8.56 us
    all_to_all x1, waiting for transfers between devices, per_device(): lax.all_to_all(outgoing, 'ep', split_axis=0, concat_axis=0, tiled=True)  7.35 us
    psum x1, blocking collectives, per_device(): lax.psum((jnp.sum(out_resid, -1), jnp.sum(out_resid * out_resid, -1)), 'tp')  5.88 us
    psum x1, blocking collectives, per_device(): lax.psum((jnp.sum(own_resid, -1), jnp.sum(own_resid * own_resid, -1)), 'tp')  5.76 us
  transfers between devices with their start and end apart: 4, of which 3 were waited for; matrix products, arithmetic and copies ran while one was open for 2% of the time, Pallas kernels for 0%

commit v1 on v0

v1 whole, which is shorter than its diff:
```python
import functools

import jax
import jax.numpy as jnp
from jax import lax
from jax.experimental import pallas as pl
from jax.experimental.pallas import tpu as pltpu
from jax.sharding import PartitionSpec as P

res_scale = 2.0**0.5
decay_tau = 16.0
norm_eps = 1e-05
AHEAD = 6
F32 = jnp.float32
BF16 = jnp.bfloat16


def dot(left, right):
    return jnp.dot(left, right, preferred_element_type=F32)


def dot_nt(left, right):
    return lax.dot_general(left, right, (((1,), (1,)), ((), ())), preferred_element_type=F32)


def iota_f(shape, dim):
    return lax.broadcasted_iota(jnp.int32, shape, dim).astype(F32)


def quotient(values, divisor):
    return jnp.floor((values + 0.5) * (1.0 / divisor))


def silu(x):
    return x * (1.0 / (1.0 + jnp.exp(-x)))


def kernel(
    dims,
    tokens,
    decay_down,
    decay_up,
    decay_bias,
    head_gain,
    norm1_gain,
    route_ids,
    route_weight,
    norm2_gain,
    state_h,
    wq_h,
    wk_h,
    wv_h,
    wg_h,
    wo_h,
    eg_h,
    eu_h,
    ed_h,
    sg_h,
    su_h,
    sd_h,
    out,
    state,
    wq,
    wk,
    wv,
    wg,
    wo,
    eg,
    eu,
    ed,
    sg,
    su,
    sd,
    dq_ref,
    att_ref,
    head_out,
    p1s,
    p1r,
    p2s,
    p2r,
    p3s,
    p3r,
    p4s,
    p4r,
    p4hs,
    p4hr,
    p5,
    p5h,
    p6s,
    p6r,
    p7s,
    p7r,
    load_sem,
    tp_send,
    tp_recv,
    ep_send,
    ep_recv,
):
    (rows, heads, kdim, vdim, cols, tp, ep, local, cap, rd, groups, fc, fsc, top, chunks) = dims
    experts = local * ep
    slots = ep * rd
    me_t = lax.axis_index("tp")
    me_e = lax.axis_index("ep")

    def tp_peer(offset):
        return lax.rem(me_t + offset, tp)

    def ep_peer(offset):
        return lax.rem(me_e + offset, ep)

    barrier = pltpu.get_barrier_semaphore()
    for offset in range(1, tp):
        pl.semaphore_signal(
            barrier, inc=1, device_id=(me_e, tp_peer(offset)), device_id_type=pl.DeviceIdType.MESH
        )
    for offset in range(1, ep):
        pl.semaphore_signal(
            barrier, inc=1, device_id=(ep_peer(offset), me_t), device_id_type=pl.DeviceIdType.MESH
        )

    loads = []

    def add_load(src, dst):
        loads.append(pltpu.make_async_copy(src, dst, load_sem.at[len(loads)]))
        return len(loads) - 1

    step = rows // chunks
    i_wq = add_load(wq_h, wq)
    i_wk = add_load(wk_h, wk)
    i_state = [
        add_load(state_h.at[pl.ds(c * step, step)], state.at[pl.ds(c * step, step)])
        for c in range(chunks)
    ]
    half = wv_h.shape[0] // 2
    i_wv = [add_load(wv_h.at[pl.ds(c * half, half)], wv.at[pl.ds(c * half, half)]) for c in range(2)]
    i_wg = [add_load(wg_h.at[pl.ds(c * half, half)], wg.at[pl.ds(c * half, half)]) for c in range(2)]
    i_wo = []
    for offset in range(tp):
        start = pl.multiple_of(tp_peer(offset + 1) * cols, 128)
        i_wo.append(add_load(wo_h.at[:, pl.ds(start, cols)], wo.at[offset]))
    i_sg = add_load(sg_h, sg)
    i_su = add_load(su_h, su)
    i_eg = add_load(eg_h, eg)
    i_eu = add_load(eu_h, eu)
    i_sd = add_load(sd_h, sd)
    i_ed = add_load(ed_h, ed)
    for copy in loads[:AHEAD]:
        copy.start()

    def ready(index):
        loads[index].wait()
        if index + AHEAD < len(loads):
            loads[index + AHEAD].start()

    def tp_copy(src, dst, kind, slot, target):
        return pltpu.make_async_remote_copy(
            src_ref=src,
            dst_ref=dst,
            send_sem=tp_send.at[kind, slot],
            recv_sem=tp_recv.at[kind, slot],
            device_id=(me_e, target),
            device_id_type=pl.DeviceIdType.MESH,
        )

    def ep_copy(src, dst, kind, slot, target):
        return pltpu.make_async_remote_copy(
            src_ref=src,
            dst_ref=dst,
            send_sem=ep_send.at[kind, slot],
            recv_sem=ep_recv.at[kind, slot],
            device_id=(target, me_t),
            device_id_type=pl.DeviceIdType.MESH,
        )

    tok = tokens[...]
    decay_low = dot(tok, decay_down[...]).astype(BF16)
    pre = dot(decay_low, decay_up[...]) + decay_bias[...]
    log_decay = (jnp.minimum(pre, 0.0) - jnp.log(1.0 + jnp.exp(-jnp.abs(pre)))) * (1.0 / decay_tau)
    ids = route_ids[...]
    weights = route_weight[...]
    expert_iota = lax.broadcasted_iota(jnp.int32, (rows, experts), 1)
    member = jnp.zeros((rows, experts), F32)
    weight_of = jnp.zeros((rows, experts), F32)
    for k in range(top):
        hit = ids[:, k : k + 1] == expert_iota
        member = jnp.where(hit, 1.0, member)
        weight_of = jnp.where(hit, weights[:, k : k + 1], weight_of)
    member_b = member.astype(BF16)
    earlier = (iota_f((rows, rows), 1) < iota_f((rows, rows), 0)).astype(F32).astype(BF16)
    rank_b = dot(earlier, member_b).astype(BF16)

    def slot_parts(number):
        dest = quotient(number, rd)
        inner = number - dest * rd
        which = quotient(inner, cap)
        return dest * local + which, inner - which * cap, which, inner < local * cap

    e_row, c_row, _, ok_row = slot_parts(iota_f((1, slots), 1))
    expand = ((iota_f((experts, slots), 0) == e_row) & ok_row).astype(F32).astype(BF16)
    e_col, c_col, _, ok_col = slot_parts(iota_f((slots, 1), 0))
    expand_t = ((iota_f((slots, experts), 1) == e_col) & ok_col).astype(F32).astype(BF16)
    place = jnp.where(
        (dot_nt(expand_t, member_b) > 0.5) & (dot_nt(expand_t, rank_b) == c_col), 1.0, 0.0
    ).astype(BF16)
    place_t = (dot(member_b, expand) > 0.5) & (dot(rank_b, expand) == c_row)
    weight_hi = weight_of.astype(BF16)
    weight_lo = (weight_of - weight_hi.astype(F32)).astype(BF16)
    gather_hi = jnp.where(place_t, dot(weight_hi, expand), 0.0).astype(BF16)
    gather_lo = jnp.where(place_t, dot(weight_lo, expand), 0.0).astype(BF16)
    row_expert = slot_parts(iota_f((slots, 1), 0))[2]

    ready(i_wq)
    queries = dot(tok, wq[...]).astype(BF16).astype(F32) * kdim ** (-0.5)
    dq_ref[...] = queries * jnp.exp(log_decay)
    ready(i_wk)
    key_rows = dot(tok, wk[...]).astype(BF16).astype(F32)
    pairs = queries * key_rows
    width = heads * kdim
    hr = att_ref.shape[1]
    head_mask = quotient(iota_f((hr, width), 1), kdim) == iota_f((hr, width), 0)
    for c in range(chunks):
        ready(i_state[c])

        def one_row(b, carry):
            left = jnp.where(head_mask, dq_ref[pl.ds(b, 1), :], 0.0).astype(BF16)
            right = state[b].reshape(width, vdim).astype(BF16)
            att_ref[b] = dot(left, right)
            return carry

        lax.fori_loop(c * step, (c + 1) * step, one_row, 0, unroll=min(step, 3))
    for i in i_wv:
        ready(i)
    values = dot(tok, wv[...]).astype(BF16).astype(F32)
    for i in i_wg:
        ready(i)
    gate_pre = dot(tok, wg[...]).astype(BF16).astype(F32)
    for h in range(heads):
        part = slice(h * vdim, (h + 1) * vdim)
        score = jnp.sum(pairs[:, h * kdim : (h + 1) * kdim], -1, keepdims=True)
        attended = att_ref[:, h, :] + score * values[:, part]
        inv = lax.rsqrt(jnp.mean(attended * attended, -1, keepdims=True) + norm_eps)
        head_out[:, part] = (attended * inv * head_gain[...] * silu(gate_pre[:, part])).astype(BF16)
    pl.semaphore_wait(barrier, tp - 1 + ep - 1)

    sent = []
    heads_side = head_out[...]
    own = None
    for offset in range(1, tp + 1):
        ready(i_wo[offset - 1])
        product = dot(heads_side, wo[offset - 1])
        if offset < tp:
            p1s[offset] = product.astype(BF16)
            copy = tp_copy(p1s.at[offset], p1r.at[offset], 0, offset, tp_peer(offset))
            copy.start()
            sent.append(copy)
        else:
            own = product
    start = pl.multiple_of(me_t * cols, 128)
    resid = own + res_scale * tokens[:, pl.ds(start, cols)].astype(F32)
    for offset in range(1, tp):
        sent[offset - 1].wait_recv()
        resid = resid + p1r[offset].astype(F32)

    def layer_norm(values, send_ref, recv_ref, kind, gain):
        mean = jnp.mean(values, -1, keepdims=True)
        center = values - mean
        moment = jnp.sum(center * center, -1, keepdims=True)
        lane = lax.broadcasted_iota(jnp.int32, (rows, 128), 1)
        send_ref[...] = jnp.where(lane == 0, mean, moment)
        copies = []
        for offset in range(1, tp):
            copy = tp_copy(send_ref, recv_ref.at[offset], kind, offset, tp_peer(offset))
            copy.start()
            copies.append(copy)
        sent.extend(copies)
        means, moments = [mean], moment
        for offset in range(1, tp):
            copies[offset - 1].wait_recv()
            tile = recv_ref[offset]
            means.append(tile[:, 0:1])
            moments = moments + tile[:, 1:2]
        total = sum(means) * (1.0 / tp)
        for m in means:
            moments = moments + cols * (m - total) * (m - total)
        return (values - total) * lax.rsqrt(moments * (1.0 / (cols * tp)) + norm_eps) * gain[...]

    normed = layer_norm(resid, p2s, p2r, 1, norm1_gain).astype(BF16)

    p3s[...] = dot(place, normed).astype(BF16).reshape(ep, rd, cols)
    routed_copies = []
    for offset in range(1, ep):
        target = ep_peer(offset)
        copy = ep_copy(p3s.at[target], p3r.at[offset], 0, offset, target)
        copy.start()
        routed_copies.append(copy)
    sent.extend(routed_copies)
    p3r[0] = p3s[me_e]

    def send_rows(send_ref, recv_ref, kind, group):
        @pl.when(me_t != group)
        def _():
            pltpu.make_async_remote_copy(
                src_ref=send_ref.at[group],
                dst_ref=recv_ref.at[me_t],
                send_sem=tp_send.at[kind, group],
                recv_sem=tp_recv.at[kind, me_t],
                device_id=(me_e, group),
                device_id_type=pl.DeviceIdType.MESH,
            ).start()

    def settle_sends(send_ref, recv_ref, kind):
        for group in range(groups):

            @pl.when(me_t != group)
            def _():
                tp_copy(send_ref.at[group], recv_ref.at[me_t], kind, group, group).wait_send()

    ready(i_sg)
    ready(i_su)
    shared_gate, shared_up = dot(normed, sg[...]), dot(normed, su[...])
    for group in range(groups):
        part = slice(group * fsc, (group + 1) * fsc)
        p4hs[group, :, 0:fsc] = shared_gate[:, part].astype(BF16)
        p4hs[group, :, fsc : 2 * fsc] = shared_up[:, part].astype(BF16)
        send_rows(p4hs, p4hr, 3, group)

    ready(i_eg)
    ready(i_eu)
    for copy in routed_copies:
        copy.wait_recv()
    incoming = p3r[...].reshape(slots, cols)
    masked = [jnp.where(row_expert == e, incoming, jnp.zeros_like(incoming)) for e in range(local)]
    for group in range(groups):
        part = slice(group * fc, (group + 1) * fc)
        gate_sum = sum(dot(masked[e], eg[e, :, part]) for e in range(local))
        up_sum = sum(dot(masked[e], eu[e, :, part]) for e in range(local))
        p4s[group, :, 0:fc] = gate_sum.astype(BF16)
        p4s[group, :, fc : 2 * fc] = up_sum.astype(BF16)
        send_rows(p4s, p4r, 2, group)

    def reduce(send_ref, recv_ref, kind, dest, kind_out, chunk):
        total = send_ref[me_t].astype(F32)
        for offset in range(1, tp):
            source = tp_peer(offset)
            tp_copy(send_ref.at[0], recv_ref.at[source], kind, source, source).wait_recv()
            total = total + recv_ref[source].astype(F32)
        dest[me_t] = (silu(total[:, 0:chunk]) * total[:, chunk : 2 * chunk]).astype(BF16)
        for offset in range(1, tp):
            pltpu.make_async_remote_copy(
                src_ref=dest.at[me_t],
                dst_ref=dest.at[me_t],
                send_sem=tp_send.at[kind_out, offset],
                recv_sem=tp_recv.at[kind_out, me_t],
                device_id=(me_e, tp_peer(offset)),
                device_id_type=pl.DeviceIdType.MESH,
            ).start()

    def all_reduce():
        reduce(p4hs, p4hr, 3, p5h, 5, fsc)
        reduce(p4s, p4r, 2, p5, 4, fc)

    def gathered(dest, kind):
        for group in range(groups):

            @pl.when(me_t != group)
            def _():
                tp_copy(dest.at[group], dest.at[group], kind, group, group).wait_recv()

    if groups == tp:
        all_reduce()
    else:
        pl.when(me_t < groups)(all_reduce)
    settle_sends(p4hs, p4hr, 3)
    settle_sends(p4s, p4r, 2)
    gathered(p5h, 5)
    ready(i_sd)
    mixture = sum(
        dot(p5h[group], sd[group * fsc : (group + 1) * fsc, :]) for group in range(groups)
    )
    ready(i_ed)
    gathered(p5, 4)
    answer = jnp.zeros((slots, cols), F32)
    for group in range(groups):
        inner = p5[group]
        for e in range(local):
            answer = answer + dot(
                jnp.where(row_expert == e, inner, jnp.zeros_like(inner)),
                ed[e, group * fc : (group + 1) * fc, :],
            )
    p6s[...] = answer.astype(BF16).reshape(ep, rd, cols)
    back_copies = []
    for offset in range(1, ep):
        source = ep_peer(ep - offset)
        copy = ep_copy(p6s.at[offset], p6r.at[ep_peer(0)], 1, offset, source)
        copy.start()
        back_copies.append(copy)
    sent.extend(back_copies)
    p6r[me_e] = p6s[0]
    for offset in range(1, ep):
        expert_dev = ep_peer(offset)
        ep_copy(p6s.at[offset], p6r.at[expert_dev], 1, offset, expert_dev).wait_recv()
    returned = p6r[...].reshape(slots, cols)
    mixture = mixture + dot(gather_hi, returned) + dot(gather_lo, returned)
    last = res_scale * normed.astype(F32) + mixture
    out[...] = layer_norm(last, p7s, p7r, 6, norm2_gain).astype(BF16)
    for copy in sent:
        copy.wait_send()

    def settle_gather(dest, kind):
        for offset in range(1, tp):
            tp_copy(dest.at[me_t], dest.at[me_t], kind, offset, tp_peer(offset)).wait_send()

    def settle_gathers():
        settle_gather(p5, 4)
        settle_gather(p5h, 5)

    if groups == tp:
        settle_gathers()
    else:
        pl.when(me_t < groups)(settle_gathers)


def per_device(
    tokens,
    state,
    w_query,
    w_key,
    w_value,
    w_outgate,
    decay_down,
    decay_up,
    decay_bias,
    head_gain,
    w_output,
    norm1_gain,
    route_ids,
    route_weight,
    exp_gate,
    exp_up,
    exp_down,
    sh_gate,
    sh_up,
    sh_down,
    norm2_gain,
):
    rows, width = tokens.shape
    heads, kdim, vdim = state.shape[1:]
    tp, ep = lax.axis_size("tp"), lax.axis_size("ep")
    cols = width // tp
    top = route_ids.shape[1]
    local = exp_gate.shape[0]
    cap = max(2, rows * top // (local * ep) + 1)
    rd = -(-local * cap // 8) * 8
    slots = ep * rd
    ff, fs = exp_gate.shape[2], sh_gate.shape[1]
    groups = min(tp, ff // 128, fs // 128)
    fc, fsc = ff // groups, fs // groups
    chunks = 4
    dims = (rows, heads, kdim, vdim, cols, tp, ep, local, cap, rd, groups, fc, fsc, top, chunks)
    n_loads = 2 + chunks + 4 + tp + 6
    vm = pltpu.VMEM
    vmem = pl.BlockSpec(memory_space=pltpu.VMEM)
    hbm = pl.BlockSpec(memory_space=pl.ANY)
    return pl.pallas_call(
        functools.partial(kernel, dims),
        out_shape=jax.ShapeDtypeStruct((rows, cols), BF16),
        in_specs=[vmem] * 9 + [hbm] * 12,
        out_specs=vmem,
        scratch_shapes=[
            vm(state.shape, F32),
            vm(w_query.shape, BF16),
            vm(w_key.shape, BF16),
            vm(w_value.shape, BF16),
            vm(w_outgate.shape, BF16),
            vm((tp, w_output.shape[0], cols), BF16),
            vm(exp_gate.shape, BF16),
            vm(exp_up.shape, BF16),
            vm(exp_down.shape, BF16),
            vm(sh_gate.shape, BF16),
            vm(sh_up.shape, BF16),
            vm(sh_down.shape, BF16),
            vm((rows, heads * kdim), F32),
            vm((rows, -(-heads // 8) * 8, vdim), F32),
            vm((rows, heads * vdim), BF16),
            vm((tp, rows, cols), BF16),
            vm((tp, rows, cols), BF16),
            vm((rows, 128), F32),
            vm((tp, rows, 128), F32),
            vm((ep, rd, cols), BF16),
            vm((ep, rd, cols), BF16),
            vm((groups, slots, 2 * fc), BF16),
            vm((tp, slots, 2 * fc), BF16),
            vm((groups, rows, 2 * fsc), BF16),
            vm((tp, rows, 2 * fsc), BF16),
            vm((groups, slots, fc), BF16),
            vm((groups, rows, fsc), BF16),
            vm((ep, rd, cols), BF16),
            vm((ep, rd, cols), BF16),
            vm((rows, 128), F32),
            vm((tp, rows, 128), F32),
            pltpu.SemaphoreType.DMA((n_loads,)),
            pltpu.SemaphoreType.DMA((7, tp)),
            pltpu.SemaphoreType.DMA((7, tp)),
            pltpu.SemaphoreType.DMA((2, ep)),
            pltpu.SemaphoreType.DMA((2, ep)),
        ],
        compiler_params=pltpu.CompilerParams(
            collective_id=0, has_side_effects=True, vmem_limit_bytes=60 * 1024 * 1024
        ),
        name="layer",
    )(
        tokens,
        decay_down,
        decay_up,
        decay_bias[None, :],
        head_gain[None, :],
        norm1_gain[None, :],
        route_ids,
        route_weight,
        norm2_gain[None, :],
        state,
        w_query,
        w_key,
        w_value,
        w_outgate,
        w_output,
        exp_gate,
        exp_up,
        exp_down,
        sh_gate,
        sh_up,
        sh_down,
    )


def solution(mesh):
    in_specs = (
        P("ep", None),
        P("ep", "tp", None, None),
        P(None, "tp"),
        P(None, "tp"),
        P(None, "tp"),
        P(None, "tp"),
        P(),
        P(None, "tp"),
        P("tp"),
        P(),
        P("tp", None),
        P("tp"),
        P("ep", None),
        P("ep", None),
        P("ep", "tp", None),
        P("ep", "tp", None),
        P("ep", None, "tp"),
        P("tp", None),
        P("tp", None),
        P(None, "tp"),
        P("tp"),
    )
    out_specs = P("ep", "tp")
    return jax.shard_map(
        per_device, mesh=mesh, in_specs=in_specs, out_specs=out_specs, check_vma=False
    )
```

time: 143 us -> 55.1 us (0.39)
  waiting for transfers between devices: 58.6 us -> 0 us
  Pallas kernels: 0 us -> 48.8 us
  matrix products: 29.9 us -> 0 us
  blocking collectives: 22.5 us -> 0 us
  between operations: 13.7 us -> 0.01 us
  starting transfers between devices: 11.3 us -> 0 us
  other arithmetic: 3.59 us -> 0 us
  local copies, waits for them, and re-layouts: 3.1 us -> 5.91 us
    pallas_call x0 -> x1, Pallas kernels: none -> 48.8 us  [per_device(): pl.pallas_call(functools.partial(kernel, dims), out_shape=jax.ShapeDtypeS...]
    dot_general x16 -> x0, matrix products: 29.9 us -> none  [the longest x10 16.4 us: project(): return jnp.dot(left, right, preferred_element_type=jnp.float32)]
    psum x1 -> x0, waiting for transfers between devices: 29.9 us -> none  [per_device(): lax.psum(up_part.astype(jnp.bfloat16), 'tp').astype(jnp.float32)]
    psum x3 -> x0, blocking collectives: 22.5 us -> none  [the longest x1 10.9 us: per_device(): lax.psum(shared_up_part.astype(jnp.bfloat16), 'tp').astype(jnp.float32)]
    reduce_scatter x1 -> x0, waiting for transfers between devices: 21.4 us -> none  [per_device(): lax.psum_scatter(partial_out.astype(jnp.bfloat16), 'tp', scatter_dimensio...]
    all_to_all x2 -> x0, starting transfers between devices: 11.2 us -> none  [the longest x1 5.67 us: per_device(): lax.all_to_all(outgoing, 'ep', split_axis=0, concat_axis=0, tiled=True)]
    all_to_all x2 -> x0, waiting for transfers between devices: 7.35 us -> none  [the longest x1 7.35 us: per_device(): lax.all_to_all(outgoing, 'ep', split_axis=0, concat_axis=0, tiled=True)]
    unnamed x26 -> x4, local copies, waits for them, and re-layouts: 0.74 us -> 5.91 us
  transfers between devices with their start and end apart: 4 -> 0, of which waited for: 3 -> 0; matrix products, arithmetic and copies ran while one was open for 2% -> 0% of each run, Pallas kernels for 0% -> 0%
where the time goes in v1:
time: 55.1 us; the launch traced here: 54.8 us
  Pallas kernels  48.8 us (89%)
  local copies, waits for them, and re-layouts  5.91 us (11%)
    pallas_call x1, Pallas kernels, per_device(): pl.pallas_call(functools.partial(kernel, dims), out_shape=jax.ShapeDtypeS...  48.8 us
    unnamed x4, local copies, waits for them, and re-layouts  5.91 us

profile of v1, /device:TPU:0, one launch (start us, length us, event | category | flops | bytes accessed | tf_op | source)
XLA Modules:
  0.0 54.8 jit_solution(5447290022954822430)
XLA Ops:
  0.0 1.4 %copy.23.route_ids = s32[24,6]{1,0:T(8,128)} copy(s32[24,6]{0,1:T(8,128)} %param.33) | data formatting | bytes 1152 | tf_op args[12]
  1.4 1.4 %copy.24.route_weight = f32[24,6]{1,0:T(8,128)} copy(f32[24,6]{0,1:T(8,128)} %param.34) | data formatting | bytes 1152 | tf_op args[13]
  2.7 1.8 %copy.22.decay_down = bf16[2048,16]{1,0:T(8,128)(2,1)} copy(bf16[2048,16]{0,1:T(8,128)(2,1)} %param.27) | data formatting | bytes 131072 | tf_op args[6]
  4.6 48.8 %layer.1 = bf16[24,512]{1,0:T(8,128)(2,1)} custom-call(bf16[24,2048]{1,0:T(8,128)(2,1)} %tokens.1, bf16[2048,16]{1,0:T(8,128)(2,1)} %copy.22.decay_down, bf16[16,512]{1,0:T(8,128)(2,1)} %decay_up.1, f32[1,512]{1,0:T(1,128)} %bitcast.4, f32[1,256]{1,0:T(1,128)} %bitcast.7, f32[1,512]{1,0:T(1,128)} %bitcast.5, s32[24,6]{1,0:T(8,128)} %copy.23.route_ids, ...), custom_call_target="tpu_custom_call" | custom-call | tf_op jit(solution)/shard_map/layer/pallas_call | solution.py:464
  53.4 1.3 %copy.26 = bf16[24,512]{1,0:T(8,128)(2,1)} copy(bf16[24,512]{1,0:T(8,128)(2,1)} %layer.1) | data formatting | bytes 49152

commit v2 on v1

--- a/solution.py
+++ b/solution.py
@@ -10,7 +10,7 @@
 res_scale = 2.0**0.5
 decay_tau = 16.0
 norm_eps = 1e-05
-AHEAD = 6
+AHEAD = 10
 F32 = jnp.float32
 BF16 = jnp.bfloat16
 
@@ -173,21 +173,22 @@
         )
 
     tok = tokens[...]
-    decay_low = dot(tok, decay_down[...]).astype(BF16)
+    decay_low = dot_nt(tok, decay_down[...]).astype(BF16)
     pre = dot(decay_low, decay_up[...]) + decay_bias[...]
     log_decay = (jnp.minimum(pre, 0.0) - jnp.log(1.0 + jnp.exp(-jnp.abs(pre)))) * (1.0 / decay_tau)
     ids = route_ids[...]
     weights = route_weight[...]
-    expert_iota = lax.broadcasted_iota(jnp.int32, (rows, experts), 1)
-    member = jnp.zeros((rows, experts), F32)
-    weight_of = jnp.zeros((rows, experts), F32)
+    expert_iota = lax.broadcasted_iota(jnp.int32, (experts, rows), 0)
+    member = jnp.zeros((experts, rows), F32)
+    weight_of = jnp.zeros((experts, rows), F32)
     for k in range(top):
-        hit = ids[:, k : k + 1] == expert_iota
+        hit = ids[k : k + 1, :] == expert_iota
         member = jnp.where(hit, 1.0, member)
-        weight_of = jnp.where(hit, weights[:, k : k + 1], weight_of)
+        weight_of = jnp.where(hit, weights[k : k + 1, :], weight_of)
     member_b = member.astype(BF16)
-    earlier = (iota_f((rows, rows), 1) < iota_f((rows, rows), 0)).astype(F32).astype(BF16)
-    rank_b = dot(earlier, member_b).astype(BF16)
+    earlier = (iota_f((rows, rows), 0) < iota_f((rows, rows), 1)).astype(F32).astype(BF16)
+    identity = (iota_f((rows, rows), 0) == iota_f((rows, rows), 1)).astype(F32).astype(BF16)
+    rank_b = dot(member_b, earlier).astype(BF16)
 
     def slot_parts(number):
         dest = quotient(number, rd)
@@ -195,19 +196,29 @@
         which = quotient(inner, cap)
         return dest * local + which, inner - which * cap, which, inner < local * cap
 
-    e_row, c_row, _, ok_row = slot_parts(iota_f((1, slots), 1))
-    expand = ((iota_f((experts, slots), 0) == e_row) & ok_row).astype(F32).astype(BF16)
     e_col, c_col, _, ok_col = slot_parts(iota_f((slots, 1), 0))
-    expand_t = ((iota_f((slots, experts), 1) == e_col) & ok_col).astype(F32).astype(BF16)
-    place = jnp.where(
-        (dot_nt(expand_t, member_b) > 0.5) & (dot_nt(expand_t, rank_b) == c_col), 1.0, 0.0
-    ).astype(BF16)
-    place_t = (dot(member_b, expand) > 0.5) & (dot(rank_b, expand) == c_row)
+    expand = ((iota_f((slots, experts), 1) == e_col) & ok_col).astype(F32).astype(BF16)
+    placed = (dot(expand, member_b) > 0.5) & (dot(expand, rank_b) == c_col)
+    place = jnp.where(placed, 1.0, 0.0).astype(BF16)
     weight_hi = weight_of.astype(BF16)
     weight_lo = (weight_of - weight_hi.astype(F32)).astype(BF16)
-    gather_hi = jnp.where(place_t, dot(weight_hi, expand), 0.0).astype(BF16)
-    gather_lo = jnp.where(place_t, dot(weight_lo, expand), 0.0).astype(BF16)
-    row_expert = slot_parts(iota_f((slots, 1), 0))[2]
+    spread_hi = jnp.where(placed, dot(expand, weight_hi), 0.0).astype(BF16)
+    spread_lo = jnp.where(placed, dot(expand, weight_lo), 0.0).astype(BF16)
+    per = ep * cap
+    packed = local * per
+
+    def packed_slot(number):
+        which = quotient(number, per)
+        inner = number - which * per
+        source = quotient(inner, cap)
+        return source * rd + which * cap + inner - source * cap
+
+    squeeze = packed_slot(iota_f((packed, slots), 0)) == iota_f((packed, slots), 1)
+    squeeze = jnp.where(squeeze, 1.0, 0.0).astype(BF16)
+    widen = packed_slot(iota_f((slots, packed), 1)) == iota_f((slots, packed), 0)
+    widen = jnp.where(widen, 1.0, 0.0).astype(BF16)
+    gather_hi = dot_nt(identity, spread_hi).astype(BF16)
+    gather_lo = dot_nt(identity, spread_lo).astype(BF16)
 
     ready(i_wq)
     queries = dot(tok, wq[...]).astype(BF16).astype(F32) * kdim ** (-0.5)
@@ -288,7 +299,7 @@
 
     p3s[...] = dot(place, normed).astype(BF16).reshape(ep, rd, cols)
     routed_copies = []
-    for offset in range(1, ep):
+    for offset in sorted(range(1, ep), key=lambda o: -min(o, ep - o)):
         target = ep_peer(offset)
         copy = ep_copy(p3s.at[target], p3r.at[offset], 0, offset, target)
         copy.start()
@@ -328,15 +339,21 @@
     ready(i_eu)
     for copy in routed_copies:
         copy.wait_recv()
-    incoming = p3r[...].reshape(slots, cols)
-    masked = [jnp.where(row_expert == e, incoming, jnp.zeros_like(incoming)) for e in range(local)]
-    for group in range(groups):
-        part = slice(group * fc, (group + 1) * fc)
-        gate_sum = sum(dot(masked[e], eg[e, :, part]) for e in range(local))
-        up_sum = sum(dot(masked[e], eu[e, :, part]) for e in range(local))
-        p4s[group, :, 0:fc] = gate_sum.astype(BF16)
-        p4s[group, :, fc : 2 * fc] = up_sum.astype(BF16)
-        send_rows(p4s, p4r, 2, group)
+    incoming = dot(squeeze, p3r[...].reshape(slots, cols))
+    chosen = [incoming[e * per : (e + 1) * per].astype(BF16) for e in range(local)]
+    slab = 2 if groups % 2 == 0 else 1
+    for first in range(0, groups, slab):
+        part = slice(first * fc, (first + slab) * fc)
+        for e in range(local):
+            at = slice(e * per, (e + 1) * per)
+            gate_sum = dot(chosen[e], eg[e, :, part])
+            up_sum = dot(chosen[e], eu[e, :, part])
+            for i in range(slab):
+                cut = slice(i * fc, (i + 1) * fc)
+                p4s[first + i, at, 0:fc] = gate_sum[:, cut].astype(BF16)
+                p4s[first + i, at, fc : 2 * fc] = up_sum[:, cut].astype(BF16)
+        for i in range(slab):
+            send_rows(p4s, p4r, 2, first + i)
 
     def reduce(send_ref, recv_ref, kind, dest, kind_out, chunk):
         total = send_ref[me_t].astype(F32)
@@ -379,17 +396,13 @@
     )
     ready(i_ed)
     gathered(p5, 4)
-    answer = jnp.zeros((slots, cols), F32)
-    for group in range(groups):
-        inner = p5[group]
-        for e in range(local):
-            answer = answer + dot(
-                jnp.where(row_expert == e, inner, jnp.zeros_like(inner)),
-                ed[e, group * fc : (group + 1) * fc, :],
-            )
-    p6s[...] = answer.astype(BF16).reshape(ep, rd, cols)
+    inner = jnp.concatenate([p5[group] for group in range(groups)], 1).astype(F32)
+    answer = jnp.concatenate(
+        [dot(inner[e * per : (e + 1) * per].astype(BF16), ed[e]) for e in range(local)], 0
+    ).astype(BF16)
+    p6s[...] = dot(widen, answer).astype(BF16).reshape(ep, rd, cols)
     back_copies = []
-    for offset in range(1, ep):
+    for offset in sorted(range(1, ep), key=lambda o: -min(o, ep - o)):
         source = ep_peer(ep - offset)
         copy = ep_copy(p6s.at[offset], p6r.at[ep_peer(0)], 1, offset, source)
         copy.start()
@@ -451,7 +464,7 @@
     local = exp_gate.shape[0]
     cap = max(2, rows * top // (local * ep) + 1)
     rd = -(-local * cap // 8) * 8
-    slots = ep * rd
+    packed = local * cap * ep
     ff, fs = exp_gate.shape[2], sh_gate.shape[1]
     groups = min(tp, ff // 128, fs // 128)
     fc, fsc = ff // groups, fs // groups
@@ -488,11 +501,11 @@
             vm((tp, rows, 128), F32),
             vm((ep, rd, cols), BF16),
             vm((ep, rd, cols), BF16),
-            vm((groups, slots, 2 * fc), BF16),
-            vm((tp, slots, 2 * fc), BF16),
+            vm((groups, packed, 2 * fc), BF16),
+            vm((tp, packed, 2 * fc), BF16),
             vm((groups, rows, 2 * fsc), BF16),
             vm((tp, rows, 2 * fsc), BF16),
-            vm((groups, slots, fc), BF16),
+            vm((groups, packed, fc), BF16),
             vm((groups, rows, fsc), BF16),
             vm((ep, rd, cols), BF16),
             vm((ep, rd, cols), BF16),
@@ -510,13 +523,13 @@
         name="layer",
     )(
         tokens,
-        decay_down,
+        decay_down.T,
         decay_up,
         decay_bias[None, :],
         head_gain[None, :],
         norm1_gain[None, :],
-        route_ids,
-        route_weight,
+        route_ids.T,
+        route_weight.T,
         norm2_gain[None, :],
         state,
         w_query,

time: 55.1 us -> 48.2 us (0.87)
  local copies, waits for them, and re-layouts: 5.91 us -> 1.35 us
  Pallas kernels: 48.8 us -> 46.6 us
    unnamed x4 -> x1, local copies, waits for them, and re-layouts: 5.91 us -> 1.35 us
    pallas_call x1, Pallas kernels: 48.8 us -> 46.6 us  [per_device(): pl.pallas_call(functools.partial(kernel, dims), out_shape=jax.ShapeDtypeS...]
where the time goes in v2:
time: 48.2 us; the launch traced here: 48 us
  Pallas kernels  46.6 us (97%)
  local copies, waits for them, and re-layouts  1.35 us (3%)
    pallas_call x1, Pallas kernels, per_device(): pl.pallas_call(functools.partial(kernel, dims), out_shape=jax.ShapeDtypeS...  46.6 us
    unnamed x1, local copies, waits for them, and re-layouts  1.35 us

profile of v2, /device:TPU:0, one launch (start us, length us, event | category | flops | bytes accessed | tf_op | source)
XLA Modules:
  0.0 48.0 jit_solution(9104490072037220510)
XLA Ops:
  0.0 46.6 %layer.1 = bf16[24,512]{1,0:T(8,128)(2,1)} custom-call(bf16[24,2048]{1,0:T(8,128)(2,1)} %tokens.1, bf16[16,2048]{1,0:T(8,128)(2,1)} %bitcast.7, bf16[16,512]{1,0:T(8,128)(2,1)} %decay_up.1, f32[1,512]{1,0:T(1,128)} %bitcast.10, f32[1,256]{1,0:T(1,128)} %bitcast.13, f32[1,512]{1,0:T(1,128)} %bitcast.11, s32[6,24]{1,0:T(8,128)} %bitcast.8, f32[6,24]{1,0:T(8,128)} %bitcast.9, ...), custom_call_target="tpu_custom_call" | custom-call | tf_op jit(solution)/shard_map/layer/pallas_call | solution.py:477
  46.6 1.3 %copy.23 = bf16[24,512]{1,0:T(8,128)(2,1)} copy(bf16[24,512]{1,0:T(8,128)(2,1)} %layer.1) | data formatting | bytes 49152
